TPU v7x, 32 devices: a whole 2x2x4 slice. The times are simulated.
32 devices in a mesh: ra: 4 (over z), cb: 4 (over y, x), dp: 2 (over core).
Axes of the slice: x: 2, y: 2, z: 4, core: 2. Of those that a mesh axis runs over, the one named last changes fastest.
Arguments:
- tokens: bfloat16 [3072, 4096], P('dp', 'ra'), may hold values from -20 to 20
- pre_gain: float32 [4096], P('ra'), may hold values from 0.1 to 1.9
- up_weight: bfloat16 [4096, 16384], P('ra', 'cb'), may hold values from -0.09375 to 0.09375
- up_bias: float32 [16384], P('cb'), may hold values from -4 to 4
- down_weight: bfloat16 [16384, 4096], P('cb', 'ra'), may hold values from -0.046875 to 0.046875
- post_gain: float32 [4096], P('ra'), may hold values from 0.1 to 1.9
Outputs:
- stream_out: bfloat16 [3072, 4096], P('dp', 'ra')
All inputs are finite; a program needn't handle non-finite values.
Results may differ from a plain program's by a relative error of at most 0.0051.
Values may be sent and summed in bfloat16 or wider, within the bound.
A program may use at most 128 MiB of HBM per device.

v0:
```python
import functools

import jax
import jax.numpy as jnp
from jax import lax
from jax.experimental import pallas as pl
from jax.experimental.pallas import tpu as pltpu
from jax.sharding import PartitionSpec as P

epsilon = 1e-06
residual_weight = 0.5
MESH = pl.DeviceIdType.MESH
LANES = 128
MOST_FLAGS = 512


def pick(rows, ra, cb):
    small = 32
    while (2 * ra + 1) * (rows // small) > MOST_FLAGS and rows % (2 * small) == 0:
        small *= 2
    large = small
    while large // cb < 32 and rows % (2 * large) == 0:
        large *= 2
    return small, large


def kernel(n, m, g, big, tokens, mine, up, down, pre_gain, bias, post_gain, out,
           xs, uw, dw, rr, hg, ys, yo, yr, os, xq, acc, po, e, inv, be,
           load_sem, right_sem, left_sem, rs_sem, hg_sem, y_send, yr_sem, o_send, out_sem, out_local,
           e_send, e_sem, be_send, be_sem):
    rows, depth = xs.shape
    width = depth * n
    units = hg.shape[2]
    few = big // m
    count, blocks, per = rows // g, rows // big, big // g
    z, c = lax.axis_index("ra"), lax.axis_index("cb")
    first, last = z == 0, z == n - 1

    def at(j, size):
        return pl.ds(pl.multiple_of(j * size, size), size)

    def remote(src, dst, send, recv, **where):
        return pltpu.make_async_remote_copy(src, dst, send, recv, device_id=where, device_id_type=MESH)

    loads = [pltpu.make_async_copy(tokens, ys, load_sem.at[0])]
    loads += [pltpu.make_async_copy(up.at[:, pl.ds(s * units, units)], uw.at[s], load_sem.at[1 + s]) for s in range(n)]
    loads += [pltpu.make_async_copy(mine.at[:, c], xq, load_sem.at[1 + n])]
    loads += [pltpu.make_async_copy(down, dw, load_sem.at[2 + n])]
    for load in loads:
        load.start()

    barrier = pltpu.get_barrier_semaphore()
    for d in range(1, n):
        pl.semaphore_signal(barrier, inc=1, device_id={"ra": lax.rem(z + d, n)}, device_id_type=MESH)
    for d in range(1, m):
        pl.semaphore_signal(barrier, inc=1, device_id={"cb": lax.rem(c + d, m)}, device_id_type=MESH)
    pl.semaphore_wait(barrier, n + m - 2)

    loads[0].wait()

    @pl.loop(0, rows // LANES)
    def _(b):
        part = at(b, LANES)
        raw = ys[part, :].astype(jnp.float32)
        xs[part, :] = (raw * pre_gain[...]).astype(jnp.bfloat16)
        total = jnp.sum(raw * raw, axis=1, keepdims=True)
        e[z, :, part] = jnp.broadcast_to(total, (LANES, LANES)).T[:8, :]

    for load in loads[1:]:
        load.wait()
    for d in range(1, n):
        remote(e.at[z], e.at[z], e_send.at[d], e_sem.at[z], ra=lax.rem(z + d, n)).start()

    def dot(a, b):
        return jnp.dot(a, b, preferred_element_type=jnp.float32)

    def to_right(src, dst, flag):
        remote(src, dst, right_sem, flag, ra=jnp.minimum(z + 1, n - 1)).start()

    def to_left(src, dst, flag):
        remote(src, dst, left_sem, flag, ra=jnp.maximum(z - 1, 0)).start()

    def arrived(ref, flag):
        pltpu.make_async_copy(ref, ref, flag).wait()

    def step(i, _):
        @pl.when(i == n - 1)
        def _():
            for d in range(1, n):
                s = lax.rem(z + d, n)
                arrived(e.at[s], e_sem.at[s])

            @pl.loop(0, rows // LANES)
            def _(b):
                part = at(b, LANES)
                total = e[0, :, part]
                for s in range(1, n):
                    total = total + e[s, :, part]
                factor = lax.rsqrt(total / width + epsilon)
                inv[part, :] = jnp.broadcast_to(factor[:1, :], (LANES, LANES)).T

        j = i - n

        @pl.when(jnp.logical_and(j >= 0, j < count))
        def _():
            here = at(j, g)
            po[...] = dot(xs[here, :], uw[z])

            @pl.when(jnp.logical_not(first))
            def _():
                arrived(rr.at[z, here], rs_sem.at[z, j])
                po[...] += rr[z, here, :].astype(jnp.float32)

            @pl.when(jnp.logical_not(last))
            def _():
                arrived(rr.at[n, here], rs_sem.at[n, j])
                po[...] += rr[n, here, :].astype(jnp.float32)

            pre = po[...] * inv[here, :1] + bias[z]
            hg[z, here, :] = jnp.square(jnp.maximum(pre, 0.0)).astype(jnp.bfloat16)

            @pl.when(jnp.logical_not(last))
            def _():
                to_right(hg.at[z, here], hg.at[z, here], hg_sem.at[z, j])

            @pl.when(jnp.logical_not(first))
            def _():
                to_left(hg.at[z, here], hg.at[z, here], hg_sem.at[z, j])

        def from_left(d, _):
            s = z - d
            j = i - n - d

            @pl.when(jnp.logical_and(j >= 0, j < count))
            def _():
                here = at(j, g)
                arrived(hg.at[s, here], hg_sem.at[s, j])

                @pl.when(jnp.logical_not(last))
                def _():
                    to_right(hg.at[s, here], hg.at[s, here], hg_sem.at[s, j])

            return 0

        def from_right(d, _):
            s = z + d
            j = i - n - d

            @pl.when(jnp.logical_and(j >= 0, j < count))
            def _():
                here = at(j, g)
                arrived(hg.at[s, here], hg_sem.at[s, j])

                @pl.when(jnp.logical_not(first))
                def _():
                    to_left(hg.at[s, here], hg.at[s, here], hg_sem.at[s, j])

            return 0

        lax.fori_loop(1, z + 1, from_left, 0)
        lax.fori_loop(1, n - z, from_right, 0)

        a = i - z

        @pl.when(jnp.logical_and(a >= 0, a < count))
        def _():
            here = at(a, g)

            def segment(k, _):
                s = n - 1 - k
                part = dot(xs[here, :], uw[s])

                @pl.when(first)
                def _():
                    rr[s, here, :] = part.astype(jnp.bfloat16)

                @pl.when(jnp.logical_not(first))
                def _():
                    arrived(rr.at[s, here], rs_sem.at[s, a])
                    rr[s, here, :] = (part + rr[s, here, :].astype(jnp.float32)).astype(jnp.bfloat16)

                to_right(rr.at[s, here], rr.at[s, here], rs_sem.at[s, a])
                return 0

            lax.fori_loop(0, n - 1 - z, segment, 0)

        b = i - (n - 1 - z)

        @pl.when(jnp.logical_and(b >= 0, b < count))
        def _():
            here = at(b, g)

            def segment(s, _):
                part = dot(xs[here, :], uw[s])

                @pl.when(last)
                def _():
                    rr[s, here, :] = part.astype(jnp.bfloat16)

                @pl.when(jnp.logical_not(last))
                def _():
                    arrived(rr.at[s, here], rs_sem.at[s, b])
                    rr[s, here, :] = (part + rr[s, here, :].astype(jnp.float32)).astype(jnp.bfloat16)

                slot = jnp.where(s == z - 1, n, s)
                to_left(rr.at[s, here], rr.at[slot, here], rs_sem.at[slot, b])
                return 0

            lax.fori_loop(0, z, segment, 0)

        t = i - (2 * n - 1)
        ready = lambda t: jnp.logical_and(jnp.logical_and(t >= 0, t < count), lax.rem(t + 1, per) == 0)

        @pl.when(ready(t))
        def _():
            j = lax.div(t, per)
            here = at(j, big)
            acc[...] = dot(hg[0, here, :], dw[0])

            @pl.loop(1, n)
            def _(s):
                acc[...] += dot(hg[s, here, :], dw[s])

            ys[here, :] = acc[...].astype(jnp.bfloat16)
            yo[at(j, few), :] = acc[at(c, few), :]
            for d in range(1, m):
                peer = lax.rem(c + d, m)
                quarter = pl.ds(pl.multiple_of(j * big + peer * few, few), few)
                remote(ys.at[quarter], yr.at[c, at(j, few)], y_send.at[d], yr_sem.at[c, j], cb=peer).start()

        t1 = t - 1

        @pl.when(ready(t1))
        def _():
            j = lax.div(t1, per)
            here = at(j, few)
            branch = yo[here, :]
            for d in range(1, m):
                peer = lax.rem(c + d, m)
                arrived(yr.at[peer, here], yr_sem.at[peer, j])
                branch = branch + yr[peer, here, :].astype(jnp.float32)
            yo[here, :] = branch
            total = jnp.sum(branch * branch, axis=1, keepdims=True)
            square = jnp.concatenate([jnp.broadcast_to(total, (few, LANES))] * (LANES // few), axis=0)
            be[z, j] = square.T[:8, :]
            for d in range(1, n):
                remote(be.at[z, j], be.at[z, j], be_send.at[d], be_sem.at[z, j], ra=lax.rem(z + d, n)).start()

        t2 = t - 2

        @pl.when(ready(t2))
        def _():
            j = lax.div(t2, per)
            here = at(j, few)
            for d in range(1, n):
                s = lax.rem(z + d, n)
                arrived(be.at[s, j], be_sem.at[s, j])
            total = be[0, j]
            for s in range(1, n):
                total = total + be[s, j]
            factor = lax.rsqrt(total / width + epsilon)
            factor = jnp.broadcast_to(factor[:1, :], (LANES, LANES)).T[:few, :1]
            kept = residual_weight * xq[j].astype(jnp.float32)
            os[here, :] = (kept + yo[here, :] * factor * post_gain[...]).astype(jnp.bfloat16)
            place = pl.ds(pl.multiple_of(j * big + c * few, few), few)
            pltpu.make_async_copy(os.at[here], out.at[place], out_local).start()
            for d in range(1, m):
                peer = lax.rem(c + d, m)
                remote(os.at[here], out.at[place], o_send.at[d], out_sem.at[c], cb=peer).start()

        return 0

    lax.fori_loop(0, count + 2 * n + 1, step, 0)

    arrived(os, out_local)
    for d in range(1, m):
        arrived(os, out_sem.at[lax.rem(c + d, m)])
        arrived(os, y_send.at[d])
        arrived(os, o_send.at[d])
    for d in range(1, n):
        arrived(e.at[0], e_send.at[d])
        arrived(be.at[0], be_send.at[d])

    @pl.when(jnp.logical_not(last))
    def _():
        arrived(hg, right_sem)

    @pl.when(jnp.logical_not(first))
    def _():
        arrived(hg, left_sem)


def solution(mesh):
    n, m = mesh.shape["ra"], mesh.shape["cb"]

    def body(tokens, pre_gain, up, bias, down, post_gain):
        rows, depth = tokens.shape
        units = up.shape[1] // n
        g, big = pick(rows, n, m)
        few, blocks, count = big // m, rows // big, rows // g
        whole = pl.BlockSpec(memory_space=pl.ANY)
        inside = pl.BlockSpec(memory_space=pltpu.VMEM)
        bf16, f32, dma = jnp.bfloat16, jnp.float32, pltpu.SemaphoreType.DMA
        return pl.pallas_call(
            functools.partial(kernel, n, m, g, big),
            out_shape=jax.ShapeDtypeStruct((rows, depth), bf16),
            in_specs=[whole] * 4 + [inside] * 3,
            out_specs=whole,
            scratch_shapes=[
                pltpu.VMEM((rows, depth), bf16),
                pltpu.VMEM((n, depth, units), bf16),
                pltpu.VMEM((n, units, depth), bf16),
                pltpu.VMEM((n + 1, rows, units), bf16),
                pltpu.VMEM((n, rows, units), bf16),
                pltpu.VMEM((rows, depth), bf16),
                pltpu.VMEM((rows // m, depth), f32),
                pltpu.VMEM((m, rows // m, depth), bf16),
                pltpu.VMEM((rows // m, depth), bf16),
                pltpu.VMEM((blocks, few, depth), bf16),
                pltpu.VMEM((big, depth), f32),
                pltpu.VMEM((g, units), f32),
                pltpu.VMEM((n, 8, rows), f32),
                pltpu.VMEM((rows, LANES), f32),
                pltpu.VMEM((n, blocks, 8, LANES), f32),
                dma((n + 3,)), dma, dma, dma((n + 1, count)), dma((n, count)),
                dma((m,)), dma((m, blocks)), dma((m,)), dma((m,)), dma,
                dma((n,)), dma((n,)), dma((n,)), dma((n, blocks)),
            ],
            compiler_params=pltpu.CompilerParams(
                collective_id=0, has_side_effects=True, vmem_limit_bytes=67043328),
            name="feed_forward",
        )(tokens, tokens.reshape(blocks, m, few, depth), up, down.reshape(n, units, depth),
          pre_gain.reshape(1, depth), bias.reshape(n, 1, units), post_gain.reshape(1, depth))

    in_specs = (P("dp", "ra"), P("ra"), P("ra", "cb"), P("cb"), P("cb", "ra"), P("ra"))
    return jax.shard_map(body, mesh=mesh, in_specs=in_specs, out_specs=P("dp", "ra"), check_vma=False)
```

profile of v0, /device:TPU:0, one launch (start us, length us, event | category | flops | bytes accessed | tf_op | source)
XLA Modules:
  0.0 327.8 jit_solution(4782464997955108744)
XLA Ops:
  0.0 324.0 %feed_forward.1 = bf16[1536,1024]{1,0:T(8,128)(2,1)} custom-call(bf16[1536,1024]{1,0:T(8,128)(2,1)} %tokens.1, bf16[12,4,32,1024]{3,2,1,0:T(8,128)(2,1)} %bitcast.5, bf16[1024,4096]{1,0:T(8,128)(2,1)} %up.1, bf16[4,1024,1024]{2,1,0:T(8,128)(2,1)} %bitcast.6, f32[1,1024]{1,0:T(1,128)} %bitcast.8, f32[4,1,1024]{2,1,0:T(1,128)} %bitcast.7, f32[1,1024]{1,0:T(1,128)} %bitcast.9), custom_call_target="tpu_custom_call" | custom-call | tf_op jit(solution)/shard_map/feed_forward/pallas_call | solution.py:304
  324.0 3.9 %copy.8 = bf16[1536,1024]{1,0:T(8,128)(2,1)} copy(bf16[1536,1024]{1,0:T(8,128)(2,1)} %feed_forward.1) | data formatting | bytes 6291456
where the time goes:
time: 328 us
  Pallas kernels  324 us (99%)
  local copies, waits for them, and re-layouts  3.86 us (1%)
    pallas_call x1, Pallas kernels, body(): pl.pallas_call(functools.partial(kernel, n, m, g, big), out_shape=jax.Sha...  324 us

commit v1 on v0

v1 whole, which is shorter than its diff:
```python
import functools

import jax
import jax.numpy as jnp
from jax import lax
from jax.experimental import pallas as pl
from jax.experimental.pallas import tpu as pltpu
from jax.sharding import PartitionSpec as P

epsilon = 1e-06
residual_weight = 0.5
MESH = pl.DeviceIdType.MESH
LANES = 128
MOST_FLAGS = 512


def pick(rows, ra, cb):
    small = 32
    while (2 * ra + (ra + 1) // 2) * (rows // small) > MOST_FLAGS and 2 * small <= LANES:
        small *= 2
    large = small
    while large // cb < 32 and rows % (2 * large) == 0:
        large *= 2
    return small, large


def kernel(n, m, g, big, tokens, mine, up, down, pre_gain, bias, post_gain, out,
           xs, uw, dw, rr, hg, ys, yo, yr, os, xq, acc, up_sum, e, inv, be,
           load_sem, right_sem, left_sem, rs_sem, hg_sem, y_send, yr_sem, o_send, out_sem, out_local,
           e_send, e_sem, be_send, be_sem):
    rows, depth = xs.shape
    width = depth * n
    units = hg.shape[2]
    few = big // m
    count, blocks, per = rows // g, rows // big, big // g
    z, c = lax.axis_index("ra"), lax.axis_index("cb")
    first, last = z == 0, z == n - 1
    half, reach = (n + 1) // 2, n // 2
    low, high = (n - 1) // 2, n // 2
    owners = sorted({low, high})
    group = LANES // g

    def at(j, size):
        return pl.ds(pl.multiple_of(j * size, size), size)

    def remote(src, dst, send, recv, **where):
        return pltpu.make_async_remote_copy(src, dst, send, recv, device_id=where, device_id_type=MESH)

    def load_up(s):
        return pltpu.make_async_copy(up.at[:, pl.ds(pl.multiple_of(s * units, units), units)], uw.at[s], load_sem.at[s])

    head, rest = pl.ds(0, LANES), pl.ds(LANES, rows - LANES)
    load_head = pltpu.make_async_copy(tokens.at[head], ys.at[head], load_sem.at[n])
    load_rest = pltpu.make_async_copy(tokens.at[rest], ys.at[rest], load_sem.at[n + 1])
    load_mine = pltpu.make_async_copy(mine.at[:, c], xq, load_sem.at[n + 2])
    load_down = pltpu.make_async_copy(down, dw, load_sem.at[n + 3])
    load_head.start()
    for d in range(n):
        load_up(jnp.where(z <= low, n - 1 - d, d)).start()
    load_rest.start()

    barrier = pltpu.get_barrier_semaphore()
    for d in range(1, n):
        pl.semaphore_signal(barrier, inc=1, device_id={"ra": lax.rem(z + d, n)}, device_id_type=MESH)
    for d in range(1, m):
        pl.semaphore_signal(barrier, inc=1, device_id={"cb": lax.rem(c + d, m)}, device_id_type=MESH)

    def scale(b):
        part = at(b, LANES)
        raw = ys[part, :].astype(jnp.float32)
        xs[part, :] = (raw * pre_gain[...]).astype(jnp.bfloat16)
        total = jnp.sum(raw * raw, axis=1, keepdims=True)
        e[z, b] = jnp.broadcast_to(total, (LANES, LANES)).T[:8, :]

    def send_energy(b):
        for k, owner in enumerate(owners):
            @pl.when(z != owner)
            def _():
                remote(e.at[z, b], e.at[z, b], e_send.at[k], e_sem.at[z, b], ra=owner).start()

    load_head.wait()
    scale(0)
    pl.semaphore_wait(barrier, n + m - 2)
    send_energy(0)

    def dot(a, b):
        return jnp.dot(a, b, preferred_element_type=jnp.float32)

    def to_right(src, dst, flag):
        remote(src, dst, right_sem, flag, ra=jnp.minimum(z + 1, n - 1)).start()

    def to_left(src, dst, flag):
        remote(src, dst, left_sem, flag, ra=jnp.maximum(z - 1, 0)).start()

    def arrived(ref, flag):
        pltpu.make_async_copy(ref, ref, flag).wait()

    def product(s, j):
        @pl.when(j == 0)
        def _():
            load_up(s).wait()

        @pl.when(lax.rem(j, group) == 0)
        def _():
            up_sum[s] = dot(xs[at(lax.div(j, group), LANES), :], uw[s])

        return up_sum[s, at(lax.rem(j, group), g), :]

    def second(s):
        return n + jnp.where(s < half, s, s - half)

    def step(i, _):
        a = i - z

        @pl.when(jnp.logical_and(a >= 0, a < count))
        def _():
            here = at(a, g)

            def segment(k, _):
                s = n - 1 - k
                part = product(s, a)

                @pl.when(first)
                def _():
                    rr[s, here, :] = part.astype(jnp.bfloat16)

                @pl.when(jnp.logical_not(first))
                def _():
                    arrived(rr.at[s, here], rs_sem.at[s, a])
                    rr[s, here, :] = (part + rr[s, here, :].astype(jnp.float32)).astype(jnp.bfloat16)

                to_right(rr.at[s, here], rr.at[s, here], rs_sem.at[s, a])
                return 0

            lax.fori_loop(0, jnp.where(z < low, n, jnp.where(z < high, n - half, 0)), segment, 0)

        b = i - (n - 1 - z)

        @pl.when(jnp.logical_and(b >= 0, b < count))
        def _():
            here = at(b, g)

            def segment(s, _):
                part = product(s, b)

                @pl.when(last)
                def _():
                    rr[s, here, :] = part.astype(jnp.bfloat16)

                @pl.when(jnp.logical_not(last))
                def _():
                    arrived(rr.at[s, here], rs_sem.at[s, b])
                    rr[s, here, :] = (part + rr[s, here, :].astype(jnp.float32)).astype(jnp.bfloat16)

                owner = jnp.where(s < half, low, high)
                slot = jnp.where(z - 1 == owner, second(s), s)
                to_left(rr.at[s, here], rr.at[slot, here], rs_sem.at[slot, b])
                return 0

            lax.fori_loop(0, jnp.where(z > high, n, jnp.where(z > low, half, 0)), segment, 0)

        j = i - reach
        begin = jnp.where(z == low, 0, jnp.where(z == high, half, n))
        end = jnp.where(z == high, n, jnp.where(z == low, half, n))

        @pl.when(jnp.logical_and(jnp.logical_and(j >= 0, j < count), begin < end))
        def _():
            here = at(j, g)

            @pl.when(lax.rem(j, group) == 0)
            def _():
                b = lax.div(j, group)
                total = jnp.zeros((8, LANES), jnp.float32)
                for d in range(n):
                    s = lax.rem(z + d, n)
                    if d > 0:
                        arrived(e.at[s, b], e_sem.at[s, b])
                    total = total + e[s, b]
                factor = lax.rsqrt(total / width + epsilon)
                inv[...] = jnp.broadcast_to(factor[:1, :], (LANES, LANES)).T

            def segment(s, _):
                pre = product(s, j)
                if low > 0:
                    arrived(rr.at[s, here], rs_sem.at[s, j])
                    pre = pre + rr[s, here, :].astype(jnp.float32)
                elif n > 1:
                    @pl.when(jnp.logical_not(first))
                    def _():
                        arrived(rr.at[s, here], rs_sem.at[s, j])
                        spot = at(lax.rem(j, group), g)
                        up_sum[s, spot, :] += rr[s, here, :].astype(jnp.float32)

                    pre = up_sum[s, at(lax.rem(j, group), g), :]
                if high < n - 1:
                    slot = second(s)
                    arrived(rr.at[slot, here], rs_sem.at[slot, j])
                    pre = pre + rr[slot, here, :].astype(jnp.float32)
                elif n > 1:
                    @pl.when(jnp.logical_not(last))
                    def _():
                        slot = second(s)
                        arrived(rr.at[slot, here], rs_sem.at[slot, j])
                        spot = at(lax.rem(j, group), g)
                        up_sum[s, spot, :] += rr[slot, here, :].astype(jnp.float32)

                    pre = up_sum[s, at(lax.rem(j, group), g), :]
                pre = pre * inv[at(lax.rem(j, group), g), :1] + bias[s]
                hg[s, here, :] = jnp.square(jnp.maximum(pre, 0.0)).astype(jnp.bfloat16)

                @pl.when(jnp.logical_not(last))
                def _():
                    to_right(hg.at[s, here], hg.at[s, here], hg_sem.at[s, j])

                @pl.when(jnp.logical_not(first))
                def _():
                    to_left(hg.at[s, here], hg.at[s, here], hg_sem.at[s, j])

                return 0

            lax.fori_loop(begin, end, segment, 0)

        def from_left(s, _):
            j = i - reach - (z - jnp.where(s < half, low, high))

            @pl.when(jnp.logical_and(j >= 0, j < count))
            def _():
                here = at(j, g)
                arrived(hg.at[s, here], hg_sem.at[s, j])

                @pl.when(jnp.logical_not(last))
                def _():
                    to_right(hg.at[s, here], hg.at[s, here], hg_sem.at[s, j])

            return 0

        def from_right(s, _):
            j = i - reach - (jnp.where(s < half, low, high) - z)

            @pl.when(jnp.logical_and(j >= 0, j < count))
            def _():
                here = at(j, g)
                arrived(hg.at[s, here], hg_sem.at[s, j])

                @pl.when(jnp.logical_not(first))
                def _():
                    to_left(hg.at[s, here], hg.at[s, here], hg_sem.at[s, j])

            return 0

        lax.fori_loop(0, jnp.where(z > high, n, jnp.where(z > low, half, 0)), from_left, 0)
        lax.fori_loop(jnp.where(z < low, 0, jnp.where(z < high, half, n)), n, from_right, 0)

        chunk = lax.div(i * g, LANES) + 1

        @pl.when(jnp.logical_and(lax.rem(i * g, LANES) == 0, chunk < rows // LANES))
        def _():
            @pl.when(i == 0)
            def _():
                load_rest.wait()
                load_mine.start()
                load_down.start()

            scale(chunk)
            send_energy(chunk)

        t = i - 2 * reach
        ready = lambda t: jnp.logical_and(jnp.logical_and(t >= 0, t < count), lax.rem(t + 1, per) == 0)

        @pl.when(ready(t))
        def _():
            j = lax.div(t, per)
            here = at(j, big)

            @pl.when(j == 0)
            def _():
                load_down.wait()

            acc[...] = dot(hg[0, here, :], dw[0])

            @pl.loop(1, n)
            def _(s):
                acc[...] += dot(hg[s, here, :], dw[s])

            ys[here, :] = acc[...].astype(jnp.bfloat16)
            yo[at(j, few), :] = acc[at(c, few), :]
            for d in range(1, m):
                peer = lax.rem(c + d, m)
                quarter = pl.ds(pl.multiple_of(j * big + peer * few, few), few)
                remote(ys.at[quarter], yr.at[c, at(j, few)], y_send.at[d], yr_sem.at[c, j], cb=peer).start()

        t1 = t - 1

        @pl.when(ready(t1))
        def _():
            j = lax.div(t1, per)
            here = at(j, few)
            branch = yo[here, :]
            for d in range(1, m):
                peer = lax.rem(c + d, m)
                arrived(yr.at[peer, here], yr_sem.at[peer, j])
                branch = branch + yr[peer, here, :].astype(jnp.float32)
            yo[here, :] = branch
            total = jnp.sum(branch * branch, axis=1, keepdims=True)
            square = jnp.concatenate([jnp.broadcast_to(total, (few, LANES))] * (LANES // few), axis=0)
            be[z, j] = square.T[:8, :]
            for d in range(1, n):
                remote(be.at[z, j], be.at[z, j], be_send.at[d], be_sem.at[z, j], ra=lax.rem(z + d, n)).start()

        t2 = t - 2

        @pl.when(ready(t2))
        def _():
            j = lax.div(t2, per)
            here = at(j, few)

            @pl.when(j == 0)
            def _():
                load_mine.wait()

            for d in range(1, n):
                s = lax.rem(z + d, n)
                arrived(be.at[s, j], be_sem.at[s, j])
            total = be[0, j]
            for s in range(1, n):
                total = total + be[s, j]
            factor = lax.rsqrt(total / width + epsilon)
            factor = jnp.broadcast_to(factor[:1, :], (LANES, LANES)).T[:few, :1]
            kept = residual_weight * xq[j].astype(jnp.float32)
            os[here, :] = (kept + yo[here, :] * factor * post_gain[...]).astype(jnp.bfloat16)
            place = pl.ds(pl.multiple_of(j * big + c * few, few), few)
            pltpu.make_async_copy(os.at[here], out.at[place], out_local).start()
            for d in range(1, m):
                peer = lax.rem(c + d, m)
                remote(os.at[here], out.at[place], o_send.at[d], out_sem.at[c], cb=peer).start()

        return 0

    lax.fori_loop(0, count + 2 * reach + 2, step, 0)

    arrived(os, out_local)
    for d in range(1, m):
        arrived(os, out_sem.at[lax.rem(c + d, m)])
        arrived(os, y_send.at[d])
        arrived(os, o_send.at[d])
    for d in range(1, n):
        arrived(be.at[0], be_send.at[d])
    for k, owner in enumerate(owners):
        @pl.when(z != owner)
        def _():
            arrived(e.at[0], e_send.at[k])

    @pl.when(jnp.logical_not(last))
    def _():
        arrived(hg, right_sem)

    @pl.when(jnp.logical_not(first))
    def _():
        arrived(hg, left_sem)


def solution(mesh):
    n, m = mesh.shape["ra"], mesh.shape["cb"]

    def body(tokens, pre_gain, up, bias, down, post_gain):
        rows, depth = tokens.shape
        units = up.shape[1] // n
        g, big = pick(rows, n, m)
        few, blocks, count = big // m, rows // big, rows // g
        whole = pl.BlockSpec(memory_space=pl.ANY)
        inside = pl.BlockSpec(memory_space=pltpu.VMEM)
        bf16, f32, dma = jnp.bfloat16, jnp.float32, pltpu.SemaphoreType.DMA
        return pl.pallas_call(
            functools.partial(kernel, n, m, g, big),
            out_shape=jax.ShapeDtypeStruct((rows, depth), bf16),
            in_specs=[whole] * 4 + [inside] * 3,
            out_specs=whole,
            scratch_shapes=[
                pltpu.VMEM((rows, depth), bf16),
                pltpu.VMEM((n, depth, units), bf16),
                pltpu.VMEM((n, units, depth), bf16),
                pltpu.VMEM((n + (n + 1) // 2, rows, units), bf16),
                pltpu.VMEM((n, rows, units), bf16),
                pltpu.VMEM((rows, depth), bf16),
                pltpu.VMEM((rows // m, depth), f32),
                pltpu.VMEM((m, rows // m, depth), bf16),
                pltpu.VMEM((rows // m, depth), bf16),
                pltpu.VMEM((blocks, few, depth), bf16),
                pltpu.VMEM((big, depth), f32),
                pltpu.VMEM((n, LANES, units), f32),
                pltpu.VMEM((n, rows // LANES, 8, LANES), f32),
                pltpu.VMEM((LANES, LANES), f32),
                pltpu.VMEM((n, blocks, 8, LANES), f32),
                dma((n + 4,)), dma, dma, dma((n + (n + 1) // 2, count)), dma((n, count)),
                dma((m,)), dma((m, blocks)), dma((m,)), dma((m,)), dma,
                dma((n,)), dma((n, rows // LANES)), dma((n,)), dma((n, blocks)),
            ],
            compiler_params=pltpu.CompilerParams(
                collective_id=0, has_side_effects=True, vmem_limit_bytes=67043328),
            name="feed_forward",
        )(tokens, tokens.reshape(blocks, m, few, depth), up, down.reshape(n, units, depth),
          pre_gain.reshape(1, depth), bias.reshape(n, 1, units), post_gain.reshape(1, depth))

    in_specs = (P("dp", "ra"), P("ra"), P("ra", "cb"), P("cb"), P("cb", "ra"), P("ra"))
    return jax.shard_map(body, mesh=mesh, in_specs=in_specs, out_specs=P("dp", "ra"), check_vma=False)
```

time: 328 us -> 320 us (0.976)
  Pallas kernels: 324 us -> 316 us
    pallas_call x1, Pallas kernels: 324 us -> 316 us  [body(): pl.pallas_call(functools.partial(kernel, n, m, g, big), out_shape=jax.Sha...]
where the time goes in v1:
time: 320 us
  Pallas kernels  316 us (99%)
  local copies, waits for them, and re-layouts  3.86 us (1%)
    pallas_call x1, Pallas kernels, body(): pl.pallas_call(functools.partial(kernel, n, m, g, big), out_shape=jax.Sha...  316 us

profile of v1, /device:TPU:0, one launch (start us, length us, event | category | flops | bytes accessed | tf_op | source)
XLA Modules:
  0.0 319.9 jit_solution(3483504726590024970)
XLA Ops:
  0.0 316.0 %feed_forward.1 = bf16[1536,1024]{1,0:T(8,128)(2,1)} custom-call(bf16[1536,1024]{1,0:T(8,128)(2,1)} %tokens.1, bf16[12,4,32,1024]{3,2,1,0:T(8,128)(2,1)} %bitcast.5, bf16[1024,4096]{1,0:T(8,128)(2,1)} %up.1, bf16[4,1024,1024]{2,1,0:T(8,128)(2,1)} %bitcast.6, f32[1,1024]{1,0:T(1,128)} %bitcast.8, f32[4,1,1024]{2,1,0:T(1,128)} %bitcast.7, f32[1,1024]{1,0:T(1,128)} %bitcast.9), custom_call_target="tpu_custom_call" | custom-call | tf_op jit(solution)/shard_map/feed_forward/pallas_call | solution.py:373
  316.0 3.9 %copy.8 = bf16[1536,1024]{1,0:T(8,128)(2,1)} copy(bf16[1536,1024]{1,0:T(8,128)(2,1)} %feed_forward.1) | data formatting | bytes 6291456

commit v2 on v1

--- a/solution.py
+++ b/solution.py
@@ -21,18 +21,22 @@
     large = small
     while large // cb < 32 and rows % (2 * large) == 0:
         large *= 2
-    return small, large
-
-
-def kernel(n, m, g, big, tokens, mine, up, down, pre_gain, bias, post_gain, out,
+    tail = large
+    while tail // 2 >= max(small, 16 * cb):
+        tail //= 2
+    return small, large, tail
+
+
+def kernel(n, m, g, big, tail, tokens, up, down, pre_gain, bias, post_gain, out,
            xs, uw, dw, rr, hg, ys, yo, yr, os, xq, acc, up_sum, e, inv, be,
            load_sem, right_sem, left_sem, rs_sem, hg_sem, y_send, yr_sem, o_send, out_sem, out_local,
            e_send, e_sem, be_send, be_sem):
     rows, depth = xs.shape
     width = depth * n
     units = hg.shape[2]
-    few = big // m
-    count, blocks, per = rows // g, rows // big, big // g
+    count = rows // g
+    whole = rows // big - 1
+    kinds = [(big, 0, whole * big // g, 0), (tail, whole * big // g, count, whole)]
     z, c = lax.axis_index("ra"), lax.axis_index("cb")
     first, last = z == 0, z == n - 1
     half, reach = (n + 1) // 2, n // 2
@@ -52,13 +56,21 @@
     head, rest = pl.ds(0, LANES), pl.ds(LANES, rows - LANES)
     load_head = pltpu.make_async_copy(tokens.at[head], ys.at[head], load_sem.at[n])
     load_rest = pltpu.make_async_copy(tokens.at[rest], ys.at[rest], load_sem.at[n + 1])
-    load_mine = pltpu.make_async_copy(mine.at[:, c], xq, load_sem.at[n + 2])
+
+    def load_mine():
+        for size, begin, stop, _ in kinds:
+            part = size // m
+
+            @pl.loop(0, (stop - begin) * g // size)
+            def _(k):
+                src = pl.ds(pl.multiple_of(begin * g + k * size + c * part, part), part)
+                dst = pl.ds(pl.multiple_of(begin * g // m + k * part, part), part)
+                pltpu.make_async_copy(tokens.at[src], xq.at[dst], load_sem.at[n + 2]).start()
+
     load_down = pltpu.make_async_copy(down, dw, load_sem.at[n + 3])
     load_head.start()
     for d in range(n):
         load_up(jnp.where(z <= low, n - 1 - d, d)).start()
-    load_rest.start()
-
     barrier = pltpu.get_barrier_semaphore()
     for d in range(1, n):
         pl.semaphore_signal(barrier, inc=1, device_id={"ra": lax.rem(z + d, n)}, device_id_type=MESH)
@@ -80,6 +92,7 @@
 
     load_head.wait()
     scale(0)
+    load_rest.start()
     pl.semaphore_wait(barrier, n + m - 2)
     send_energy(0)
 
@@ -108,6 +121,81 @@
 
     def second(s):
         return n + jnp.where(s < half, s, s - half)
+
+    def finish(t, size, begin, stop, index):
+        part, steps = size // m, size // g
+
+        def ready(t):
+            inside = jnp.logical_and(t >= begin, t < stop)
+            return jnp.logical_and(inside, lax.rem(t - begin + 1, steps) == 0)
+
+        def block(t):
+            k = lax.div(t - begin, steps)
+            mine = pl.ds(pl.multiple_of(begin * g // m + k * part, part), part)
+            return index + k, begin * g + k * size, mine
+
+        def share(first_row, who):
+            return pl.ds(pl.multiple_of(first_row + who * part, part), part)
+
+        @pl.when(ready(t))
+        def _():
+            j, row, here = block(t)
+            every = pl.ds(pl.multiple_of(row, size), size)
+
+            @pl.when(j == 0)
+            def _():
+                load_down.wait()
+
+            acc[:size, :] = dot(hg[0, every, :], dw[0])
+
+            @pl.loop(1, n)
+            def _(s):
+                acc[:size, :] += dot(hg[s, every, :], dw[s])
+
+            ys[every, :] = acc[:size, :].astype(jnp.bfloat16)
+            yo[here, :] = acc[share(0, c), :]
+            for d in range(1, m):
+                peer = lax.rem(c + d, m)
+                remote(ys.at[share(row, peer)], yr.at[c, here], y_send.at[d], yr_sem.at[c, j], cb=peer).start()
+
+        @pl.when(ready(t - 1))
+        def _():
+            j, _, here = block(t - 1)
+            branch = yo[here, :]
+            for d in range(1, m):
+                peer = lax.rem(c + d, m)
+                arrived(yr.at[peer, here], yr_sem.at[peer, j])
+                branch = branch + yr[peer, here, :].astype(jnp.float32)
+            yo[here, :] = branch
+            total = jnp.sum(branch * branch, axis=1, keepdims=True)
+            square = jnp.concatenate([jnp.broadcast_to(total, (part, LANES))] * (LANES // part), axis=0)
+            be[z, j] = square.T[:8, :]
+            for d in range(1, n):
+                remote(be.at[z, j], be.at[z, j], be_send.at[d], be_sem.at[z, j], ra=lax.rem(z + d, n)).start()
+
+        @pl.when(ready(t - 2))
+        def _():
+            j, row, here = block(t - 2)
+
+            @pl.when(j == 0)
+            def _():
+                arrived(xq, load_sem.at[n + 2])
+
+            kept = residual_weight * xq[here, :].astype(jnp.float32)
+            for d in range(1, n):
+                s = lax.rem(z + d, n)
+                arrived(be.at[s, j], be_sem.at[s, j])
+            total = be[0, j]
+            for s in range(1, n):
+                total = total + be[s, j]
+            factor = lax.rsqrt(total / width + epsilon)
+            factor = jnp.broadcast_to(factor[:1, :], (LANES, LANES)).T[:part, :1]
+            os[here, :] = (kept + yo[here, :] * factor * post_gain[...]).astype(jnp.bfloat16)
+            place = share(row, c)
+            pltpu.make_async_copy(os.at[here], out.at[place], out_local).start()
+            for d in range(1, m):
+                peer = lax.rem(c + d, m)
+                remote(os.at[here], out.at[place], o_send.at[d], out_sem.at[c], cb=peer).start()
 
     def step(i, _):
         a = i - z
@@ -258,81 +346,14 @@
             @pl.when(i == 0)
             def _():
                 load_rest.wait()
-                load_mine.start()
+                load_mine()
                 load_down.start()
 
             scale(chunk)
             send_energy(chunk)
 
-        t = i - 2 * reach
-        ready = lambda t: jnp.logical_and(jnp.logical_and(t >= 0, t < count), lax.rem(t + 1, per) == 0)
-
-        @pl.when(ready(t))
-        def _():
-            j = lax.div(t, per)
-            here = at(j, big)
-
-            @pl.when(j == 0)
-            def _():
-                load_down.wait()
-
-            acc[...] = dot(hg[0, here, :], dw[0])
-
-            @pl.loop(1, n)
-            def _(s):
-                acc[...] += dot(hg[s, here, :], dw[s])
-
-            ys[here, :] = acc[...].astype(jnp.bfloat16)
-            yo[at(j, few), :] = acc[at(c, few), :]
-            for d in range(1, m):
-                peer = lax.rem(c + d, m)
-                quarter = pl.ds(pl.multiple_of(j * big + peer * few, few), few)
-                remote(ys.at[quarter], yr.at[c, at(j, few)], y_send.at[d], yr_sem.at[c, j], cb=peer).start()
-
-        t1 = t - 1
-
-        @pl.when(ready(t1))
-        def _():
-            j = lax.div(t1, per)
-            here = at(j, few)
-            branch = yo[here, :]
-            for d in range(1, m):
-                peer = lax.rem(c + d, m)
-                arrived(yr.at[peer, here], yr_sem.at[peer, j])
-                branch = branch + yr[peer, here, :].astype(jnp.float32)
-            yo[here, :] = branch
-            total = jnp.sum(branch * branch, axis=1, keepdims=True)
-            square = jnp.concatenate([jnp.broadcast_to(total, (few, LANES))] * (LANES // few), axis=0)
-            be[z, j] = square.T[:8, :]
-            for d in range(1, n):
-                remote(be.at[z, j], be.at[z, j], be_send.at[d], be_sem.at[z, j], ra=lax.rem(z + d, n)).start()
-
-        t2 = t - 2
-
-        @pl.when(ready(t2))
-        def _():
-            j = lax.div(t2, per)
-            here = at(j, few)
-
-            @pl.when(j == 0)
-            def _():
-                load_mine.wait()
-
-            for d in range(1, n):
-                s = lax.rem(z + d, n)
-                arrived(be.at[s, j], be_sem.at[s, j])
-            total = be[0, j]
-            for s in range(1, n):
-                total = total + be[s, j]
-            factor = lax.rsqrt(total / width + epsilon)
-            factor = jnp.broadcast_to(factor[:1, :], (LANES, LANES)).T[:few, :1]
-            kept = residual_weight * xq[j].astype(jnp.float32)
-            os[here, :] = (kept + yo[here, :] * factor * post_gain[...]).astype(jnp.bfloat16)
-            place = pl.ds(pl.multiple_of(j * big + c * few, few), few)
-            pltpu.make_async_copy(os.at[here], out.at[place], out_local).start()
-            for d in range(1, m):
-                peer = lax.rem(c + d, m)
-                remote(os.at[here], out.at[place], o_send.at[d], out_sem.at[c], cb=peer).start()
+        for kind in kinds:
+            finish(i - 2 * reach, *kind)
 
         return 0
 
@@ -365,15 +386,15 @@
     def body(tokens, pre_gain, up, bias, down, post_gain):
         rows, depth = tokens.shape
         units = up.shape[1] // n
-        g, big = pick(rows, n, m)
-        few, blocks, count = big // m, rows // big, rows // g
+        g, big, tail = pick(rows, n, m)
+        blocks, count = rows // big - 1 + big // tail, rows // g
         whole = pl.BlockSpec(memory_space=pl.ANY)
         inside = pl.BlockSpec(memory_space=pltpu.VMEM)
         bf16, f32, dma = jnp.bfloat16, jnp.float32, pltpu.SemaphoreType.DMA
         return pl.pallas_call(
-            functools.partial(kernel, n, m, g, big),
+            functools.partial(kernel, n, m, g, big, tail),
             out_shape=jax.ShapeDtypeStruct((rows, depth), bf16),
-            in_specs=[whole] * 4 + [inside] * 3,
+            in_specs=[whole] * 3 + [inside] * 3,
             out_specs=whole,
             scratch_shapes=[
                 pltpu.VMEM((rows, depth), bf16),
@@ -385,7 +406,7 @@
                 pltpu.VMEM((rows // m, depth), f32),
                 pltpu.VMEM((m, rows // m, depth), bf16),
                 pltpu.VMEM((rows // m, depth), bf16),
-                pltpu.VMEM((blocks, few, depth), bf16),
+                pltpu.VMEM((rows // m, depth), bf16),
                 pltpu.VMEM((big, depth), f32),
                 pltpu.VMEM((n, LANES, units), f32),
                 pltpu.VMEM((n, rows // LANES, 8, LANES), f32),
@@ -398,7 +419,7 @@
             compiler_params=pltpu.CompilerParams(
                 collective_id=0, has_side_effects=True, vmem_limit_bytes=67043328),
             name="feed_forward",
-        )(tokens, tokens.reshape(blocks, m, few, depth), up, down.reshape(n, units, depth),
+        )(tokens, up, down.reshape(n, units, depth),
           pre_gain.reshape(1, depth), bias.reshape(n, 1, units), post_gain.reshape(1, depth))
 
     in_specs = (P("dp", "ra"), P("ra"), P("ra", "cb"), P("cb"), P("cb", "ra"), P("ra"))

time: 320 us -> 319 us (level)
  no operation moved by 1% of the time
where the time goes in v2:
time: 319 us
  Pallas kernels  315 us (99%)
  local copies, waits for them, and re-layouts  3.86 us (1%)
    pallas_call x1, Pallas kernels, body(): pl.pallas_call(functools.partial(kernel, n, m, g, big, tail), out_shape=j...  315 us

profile of v2, /device:TPU:0, one launch (start us, length us, event | category | flops | bytes accessed | tf_op | source)
XLA Modules:
  0.0 318.9 jit_solution(8840120640882581918)
XLA Ops:
  0.0 315.0 %feed_forward.1 = bf16[1536,1024]{1,0:T(8,128)(2,1)} custom-call(bf16[1536,1024]{1,0:T(8,128)(2,1)} %tokens.1, bf16[1024,4096]{1,0:T(8,128)(2,1)} %up.1, bf16[4,1024,1024]{2,1,0:T(8,128)(2,1)} %bitcast.4, f32[1,1024]{1,0:T(1,128)} %bitcast.6, f32[4,1,1024]{2,1,0:T(1,128)} %bitcast.5, f32[1,1024]{1,0:T(1,128)} %bitcast.7), custom_call_target="tpu_custom_call" | custom-call | tf_op jit(solution)/shard_map/feed_forward/pallas_call | solution.py:394
  315.0 3.9 %copy.8 = bf16[1536,1024]{1,0:T(8,128)(2,1)} copy(bf16[1536,1024]{1,0:T(8,128)(2,1)} %feed_forward.1) | data formatting | bytes 6291456
